TPU v7x, 256 devices: a 4x2x16 block of a 4x16x16 slice. The times are simulated.
256 devices in a mesh: grp: 2 (over y), ep: 64 (over z, x), tp: 2 (over core).
Axes of the slice: x: 4, y: 2, z: 16, core: 2. Of those that a mesh axis runs over, the one named last changes fastest.
The devices are a block of a 4x16x16 slice.
Arguments:
- fresh_inputs: bfloat16 [2048, 2048], P(('grp', 'ep')), parts along dimension 0, may hold values from -6 to 6
- memory_arrays: float32 [2048, 32, 64, 64], P(('grp', 'ep'), 'tp'), parts along dimension 0, may hold values from -4 to 4
- chosen_specialist: int32 [2048, 2], P(('grp', 'ep')), parts along dimension 0, may hold values from 0 to 3, all different within a row; in each aligned block of 1024 rows (0 to 1023, 1024 to 2047, ...) at most 768 rows name the same one
- chosen_coefficient: bfloat16 [2048, 2], P(('grp', 'ep')), parts along dimension 0, may hold values from 0.25 to 1
- first_rescale: float32 [2048], replicated, may hold values from 0.1 to 1.9
- second_rescale: float32 [2048], replicated, may hold values from 0.1 to 1.9
- receiver_projector: bfloat16 [2048, 2048], P('tp', 'ep'), may hold values from -0.125 to 0.125
- address_projector: bfloat16 [2048, 2048], P('tp', 'ep'), may hold values from -0.125 to 0.125
- content_projector: bfloat16 [2048, 2048], P('tp', 'ep'), may hold values from -0.125 to 0.125
- final_projector: bfloat16 [2048, 2048], P('tp', 'ep'), may hold values from -0.125 to 0.125
- forget_narrowing: bfloat16 [2048, 64], replicated, may hold values from -0.125 to 0.125
- forget_widening: bfloat16 [64, 2048], P(None, 'tp'), may hold values from -0.75 to 0.75
- forget_bias: float32 [2048], P('tp'), may hold values from -3 to 1
- learning_narrowing: bfloat16 [2048, 64], replicated, may hold values from -0.125 to 0.125
- learning_widening: bfloat16 [64, 2048], P(None, 'tp'), may hold values from -0.75 to 0.75
- learning_bias: float32 [2048], P('tp'), may hold values from -1.5 to 1.5
- lane_scaling: float32 [2048], P('tp'), may hold values from 0.1 to 1.9
- instant_reward: float32 [32, 64], P('tp'), may hold values from -0.5 to 0.5
- specialist_switch: bfloat16 [2048, 28672], P(None, ('ep', 'tp')), may hold values from -0.125 to 0.125
- specialist_expand: bfloat16 [2048, 28672], P(None, ('ep', 'tp')), may hold values from -0.125 to 0.125
- specialist_contract: bfloat16 [28672, 2048], P(('ep', 'tp')), may hold values from -0.0625 to 0.0625
- common_activator: bfloat16 [2048, 5632], P(None, ('ep', 'tp')), may hold values from -0.125 to 0.125
- common_expand: bfloat16 [2048, 5632], P(None, ('ep', 'tp')), may hold values from -0.125 to 0.125
- common_contract: bfloat16 [5632, 2048], P(('ep', 'tp')), may hold values from -0.078125 to 0.078125
- common_switch: bfloat16 [2048], replicated, may hold values from -0.125 to 0.125
Outputs:
- new_tokens: bfloat16 [2048, 2048], P(('grp', 'ep', 'tp')), parts along dimension 0
- memory_after: float32 [2048, 32, 64, 64], P(('grp', 'ep'), 'tp'), parts along dimension 0
There are 2 independent parts, one for each index of `grp`. A program takes and returns all parts, laid end to end along the dimension named above; an argument that names none is the same for every part. Nothing has to cross between parts.
Inputs may be any that keep to these rules, and one draw needn't show every extreme that they name: `chosen_specialist`: each row names 2 different experts. Over the whole batch no expert is named by more than 768 rows, and in every draw some expert is named by exactly 768 rows.
All inputs are finite; a program needn't handle non-finite values.
Results may differ from a plain program's by a relative error of at most 0.014.
Values may be sent and summed in bfloat16 or wider, within the bound.
No kernel may reach another device: no remote copies, remote signals or barrier semaphores. Data moves between devices by JAX's collectives and lax.ppermute only.
A program may use at most 128 MiB of HBM per device.

v0:
```python
import jax
import jax.numpy as jnp
from jax import lax
from jax.sharding import Mesh
from jax.sharding import PartitionSpec as P

LANE_WIDTH = 64
FF_E = 7168
EP = ("ep_0", "ep_1")
GRP_EP = ("grp", "ep_0", "ep_1")
EP_TP = ("ep_0", "ep_1", "tp")
GRP_EP_TP = ("grp", "ep_0", "ep_1", "tp")
RMS_EPS = 1e-06
GROUP_EPS = 0.00064
HIGHEST = lax.Precision.HIGHEST


def turned_gather(arrays, axis, dims):
    turned = [jnp.moveaxis(a, dim, 0) for a, dim in zip(arrays, dims)]
    widths = [t[0].size for t in turned]
    both = jnp.concatenate([t.reshape(-1, w) for t, w in zip(turned, widths)], axis=1)
    whole = lax.all_gather(both, axis, axis=0, tiled=True)
    blocks = jnp.split(whole, [sum(widths[:k]) for k in range(1, len(widths))], axis=1)
    return tuple(
        (
            jnp.moveaxis(b.reshape(-1, *t.shape[1:]), 0, dim)
            for b, t, dim in zip(blocks, turned, dims)
        )
    )


def from_everyone(value, axis):
    copies = jnp.broadcast_to(value, (lax.axis_size(axis), *value.shape))
    return lax.all_to_all(copies, axis, split_axis=0, concat_axis=0, tiled=True)


def of_everyone(value, axis):
    return from_everyone(value, axis).astype(jnp.float32).sum(axis=0)


def whole_of(value, axes, dim):
    if not axes:
        return value
    nearer = lax.all_gather(value, axes[-1], axis=dim, tiled=True)
    return whole_of(nearer, axes[:-1], dim)


def side_by_side(arrays, axis, dim, along):
    ends, at = ([], 0)
    for a in arrays[:-1]:
        at += a.shape[along]
        ends.append(at)
    both = jnp.concatenate(arrays, axis=along)
    return tuple(jnp.split(lax.all_gather(both, axis, axis=dim, tiled=True), ends, axis=along))


def in_order(blocks, dim):
    dims = list(blocks.shape[1:])
    dims[dim] *= blocks.shape[0]
    return jnp.moveaxis(blocks, 0, dim).reshape(dims)


def one_gather(arrays, axis, dims):
    ravelled = jnp.concatenate([a.reshape(-1) for a in arrays])
    lines, at, finished = (lax.all_gather(ravelled, axis), 0, [])
    for a, dim in zip(arrays, dims):
        blocks = lines[:, at : at + a.size].reshape(-1, *a.shape)
        finished.append(in_order(blocks, dim))
        at += a.size
    return tuple(finished)


def cut_along(value, dim, devices):
    dims = value.shape
    blocks = value.reshape(*dims[:dim], devices, dims[dim] // devices, *dims[dim + 1 :])
    return jnp.moveaxis(blocks, dim, 0)


def sent_and_summed(value, axis, dim):
    devices = lax.axis_size(axis)
    blocks = lax.all_to_all(cut_along(value, dim, devices), axis, 0, 0, tiled=True)
    return jnp.sum(blocks.astype(jnp.float32), axis=0)


def rms_norm(values, norm_gain):
    mean_sq = jnp.mean(values * values, axis=-1, keepdims=True)
    return values * lax.rsqrt(mean_sq + RMS_EPS) * norm_gain


def widen(rounded):
    return lax.optimization_barrier(rounded).astype(jnp.float32)


def evolve_memory(
    memory_arrays,
    receiver_lanes,
    address_lanes,
    content_lanes,
    forget_lanes,
    learning_lanes,
    lane_rescale,
    instant_reward,
):
    unit_key = address_lanes * lax.rsqrt(
        jnp.sum(address_lanes * address_lanes, axis=-1, keepdims=True) + 1.0
    )
    stepped_address = address_lanes * learning_lanes
    removal = jnp.einsum("bhvk,bhk->bhv", memory_arrays, unit_key, precision=HIGHEST)
    memory_after = (
        memory_arrays * forget_lanes[:, :, None, :]
        - removal[..., None] * (unit_key * learning_lanes)[:, :, None, :]
        + content_lanes[..., None] * stepped_address[:, :, None, :]
    )
    memory_retrieval = jnp.einsum("bhvk,bhk->bhv", memory_after, receiver_lanes, precision=HIGHEST)
    centred = memory_retrieval - jnp.mean(memory_retrieval, axis=-1, keepdims=True)
    unit_address = centred * lax.rsqrt(
        jnp.mean(centred * centred, axis=-1, keepdims=True) + GROUP_EPS
    )
    instant_extra = (
        jnp.sum(receiver_lanes * stepped_address * instant_reward, axis=-1, keepdims=True)
        * content_lanes
    )
    return (memory_after, unit_address * lane_rescale + instant_extra)


def swiglu(rows_in, gate_w, up_w):
    gate_val = jnp.dot(rows_in, gate_w, preferred_element_type=jnp.float32)
    up_val = jnp.dot(rows_in, up_w, preferred_element_type=jnp.float32)
    return (jax.nn.silu(gate_val) * up_val).astype(jnp.bfloat16)


def body(
    fresh_inputs,
    memory_arrays,
    chosen_specialist,
    chosen_coefficient,
    first_rescale,
    second_rescale,
    receiver_projector,
    address_projector,
    content_projector,
    final_projector,
    forget_narrowing,
    forget_widening,
    forget_bias,
    learning_narrowing,
    learning_widening,
    learning_bias,
    lane_scaling,
    instant_reward,
    specialist_switch,
    specialist_expand,
    specialist_contract,
    common_activator,
    common_expand,
    common_contract,
    common_switch,
):
    own_rows = fresh_inputs.shape[0]
    model_width = fresh_inputs.shape[1]
    tp_count = lax.axis_size("tp")
    tp_rank = lax.axis_index("tp")
    half_width = model_width // tp_count
    head_count = half_width // LANE_WIDTH
    residual = fresh_inputs.astype(jnp.float32)
    normed = rms_norm(residual, first_rescale).astype(jnp.bfloat16)
    normed_half = lax.dynamic_slice_in_dim(normed, tp_rank * half_width, half_width, 1)
    pieces = turned_gather(
        (receiver_projector, address_projector, content_projector), EP, (1, 1, 1)
    )
    partials = tuple(
        (
            jnp.dot(normed_half, weight_block, preferred_element_type=jnp.float32)
            for weight_block in pieces
        )
    )
    partial_value = jnp.stack(partials, axis=1).astype(jnp.bfloat16)
    projected = (
        of_everyone(widen(partial_value).astype(jnp.bfloat16), "tp")
        .astype(jnp.float32)
        .astype(jnp.bfloat16)
    )
    mine = lax.dynamic_slice_in_dim(projected, tp_rank * half_width, half_width, 2)

    def divide_lanes(channels):
        return channels.astype(jnp.float32).reshape(own_rows, head_count, LANE_WIDTH)

    decay_mid = jnp.tanh(
        jnp.dot(normed, forget_narrowing, preferred_element_type=jnp.float32)
    ).astype(jnp.bfloat16)
    decay_pre = forget_bias + jnp.dot(
        decay_mid, forget_widening, preferred_element_type=jnp.float32
    )
    decay_vals = jnp.exp(-jnp.exp(-jax.nn.softplus(-decay_pre) - 0.5))
    rate_mid = jnp.dot(normed, learning_narrowing, preferred_element_type=jnp.float32).astype(
        jnp.bfloat16
    )
    rate_vals = jax.nn.sigmoid(
        learning_bias + jnp.dot(rate_mid, learning_widening, preferred_element_type=jnp.float32)
    )
    memory_after, memory_retrieval = evolve_memory(
        memory_arrays,
        divide_lanes(mine[:, 0]),
        divide_lanes(mine[:, 1]),
        divide_lanes(mine[:, 2]),
        divide_lanes(decay_vals),
        divide_lanes(rate_vals),
        lane_scaling.reshape(head_count, LANE_WIDTH),
        instant_reward,
    )
    attended = memory_retrieval.reshape(own_rows, half_width).astype(jnp.bfloat16)
    out_part = jnp.dot(
        attended, whole_of(final_projector, EP, 1), preferred_element_type=jnp.float32
    ).astype(jnp.bfloat16)
    mixed_out = (
        of_everyone(widen(out_part).astype(jnp.bfloat16), "tp")
        .astype(jnp.float32)
        .astype(jnp.bfloat16)
    )
    residual = residual + mixed_out.astype(jnp.float32)
    ffn_in = rms_norm(residual, second_rescale).astype(jnp.bfloat16)
    all_in, all_weight, all_ids = (
        *side_by_side((ffn_in, chosen_coefficient), EP, 0, 1),
        lax.all_gather(chosen_specialist, EP, axis=0, tiled=True),
    )
    column_count = specialist_switch.shape[1]
    flat_rank = lax.axis_index(EP) * tp_count + tp_rank
    expert = flat_rank * column_count // FF_E
    expert_share = jnp.sum(
        jnp.where(all_ids == expert, all_weight.astype(jnp.float32), 0.0), axis=1
    )
    hidden = swiglu(all_in, specialist_switch, specialist_expand)
    shared_hidden = swiglu(all_in, common_activator, common_expand)
    branch_scale = jax.nn.sigmoid(
        jnp.dot(all_in, common_switch, preferred_element_type=jnp.float32)
    )
    rows_mine = own_rows // tp_count
    hidden_pair, shared_pair = one_gather((hidden, shared_hidden), "tp", (1, 1))
    down_half, shared_half = (
        lax.all_to_all(specialist_contract, "tp", split_axis=1, concat_axis=0, tiled=True),
        lax.all_to_all(common_contract, "tp", split_axis=1, concat_axis=0, tiled=True),
    )
    half_total = expert_share[:, None] * jnp.dot(
        hidden_pair, down_half, preferred_element_type=jnp.float32
    )
    half_total = half_total + branch_scale[:, None] * jnp.dot(
        shared_pair, shared_half, preferred_element_type=jnp.float32
    )
    half_rows = sent_and_summed(half_total.astype(jnp.bfloat16), EP, 0)
    routed = lax.all_to_all(half_rows, "tp", split_axis=0, concat_axis=1, tiled=True)
    own_residual = lax.dynamic_slice_in_dim(residual, tp_rank * rows_mine, rows_mine, 0)
    return ((own_residual + routed).astype(jnp.bfloat16), memory_after)


def solution(mesh):
    torus = Mesh(
        mesh.devices.reshape(mesh.shape["grp"], 16, 4, mesh.shape["tp"]),
        ("grp", "ep_0", "ep_1", "tp"),
    )
    return jax.shard_map(
        body,
        mesh=torus,
        in_specs=(
            P(GRP_EP, None),
            P(GRP_EP, "tp", None, None),
            P(GRP_EP, None),
            P(GRP_EP, None),
            P(),
            P(),
            P("tp", EP),
            P("tp", EP),
            P("tp", EP),
            P("tp", EP),
            P(),
            P(None, "tp"),
            P("tp"),
            P(),
            P(None, "tp"),
            P("tp"),
            P("tp"),
            P("tp", None),
            P(None, EP_TP),
            P(None, EP_TP),
            P(EP_TP, None),
            P(None, EP_TP),
            P(None, EP_TP),
            P(EP_TP, None),
            P(),
        ),
        out_specs=(P(GRP_EP_TP, None), P(GRP_EP, "tp", None, None)),
        check_vma=False,
    )
```

profile of v0, /device:TPU:33, one launch (start us, length us, event | category | flops | bytes accessed | tf_op | source)
XLA Modules:
  0.0 657.6 jit_solution(10418199914732399732)
XLA Ops:
  7.3 1.7 pad_maximum_fusion.1
  9.1 12.9 %all_gather.22 = bf16[1024,128]{0,1:T(8,128)(2,1)} all-gather(bf16[1024,32]{0,1:T(8,128)(2,1)} %param.34), channel_id=1, replica_groups=mesh['grp'=2,'ep_0'=16,'ep_1'=4,'tp'=2] {'ep_1'}, dimensions={1}, use_global_device_ids=true | all-gather | bytes 327680 | tf_op jit(solution)/shard_map/all_gather | solution.py:44
  25.5 1.4 fusion.55
  26.9 1.4 fusion.71
  28.5 161.8 %all-gather.7.cloned.1.call-done = bf16[2048,3072]{1,0:T(8,128)(2,1)} async-done(((bf16[32,3072]{1,0:T(8,128)(2,1)}), bf16[2048,3072]{1,0:T(8,128)(2,1)}) %all-gather.7.cloned.1.call-update) | async-done | bytes 12582928 | tf_op jit(solution)/shard_map/all_gather | solution.py:22
  190.3 3.4 fusion.18
  193.6 3.5 fusion.21
  197.1 3.4 fusion.24
  200.6 6.9 %all_to_all.66 = bf16[2,16,3,2048]{3,1,2,0:T(8,128)(2,1)S(1)} all-to-all(bf16[2,16,3,2048]{3,1,2,0:T(8,128)(2,1)S(1)} %broadcast_in_dim.7), channel_id=1, replica_groups=mesh['grp'=2,'ep_0'=16,'ep_1'=4,'tp'=2] {'tp'}, dimensions={0} | all-to-all | bytes 786432 | tf_op jit(solution)/shard_map/all_to_all | solution.py:34
  208.2 15.4 %fusion.80 = f32[16,16,1,64]{3,2,1,0:T(1,128)S(1)} fusion(f32[16,16,64,1]{2,3,1,0:T(1,128)S(1)} %bitcast.83, f32[16,16,64,64]{3,2,1,0:T(8,128)} %param.26), kind=kOutput, calls=%fused_computation.96 | convolution fusion | flops 12582912 | bytes 4325376 | tf_op jit(solution)/shard_map/bhvk,bhk->bhv/dot_general | solution.py:108
  223.6 8.8 %multiply_add_fusion = f32[16,16,64,64]{3,2,1,0:T(8,128)S(1)} fusion(f32[16,16,64,64]{3,2,1,0:T(8,128)} %param.26, f32[16,16,64]{2,1,0:T(8,128)S(1)} %get-tuple-element.8, f32[16,16,64]{2,1,0:T(8,128)S(1)} %reshape.133, f32[16,16,64]{2,1,0:T(8,128)S(1)} %get-tuple-element.6, f32[16,16,64]{2,1,0:T(8,128)S(1)} %bitcast.82, f32[16,16,64]{2,1,0:T(8,128)S(1)} %mul.210), kind=kLoop, calls=%fused_computation.1 | loop fusion | flops 5242880 | bytes 8716288 | tf_op jit(solution)/shard_map/add | solution.py:110
  232.4 6.6 %fusion.81 = f32[16,16,1,64]{3,2,1,0:T(1,128)S(1)} fusion(f32[16,16,64,64]{3,2,1,0:T(8,128)S(1)} %multiply_add_fusion, bf16[16,16,64,1]{2,3,1,0:T(2,128)(2,1)S(1)} %reshape.148), kind=kOutput, calls=%fused_computation.97 | convolution fusion | flops 12582912 | bytes 4292608 | tf_op jit(solution)/shard_map/bhvk,bhk->bhv/dot_general | solution.py:114
  240.0 16.9 %all-gather.9.cloned.1.call-done = bf16[1024,2048]{0,1:T(8,128)(2,1)} async-done(((bf16[1024,128]{0,1:T(8,128)(2,1)}), bf16[1024,2048]{0,1:T(8,128)(2,1)}) %all-gather.9.cloned.1.call-update) | async-done | bytes 4194320 | tf_op jit(solution)/shard_map/all_gather | solution.py:44
  257.0 3.4 convolution_convert_fusion
  260.4 13.1 %all_to_all.67 = bf16[2,16,2048]{2,1,0:T(8,128)(2,1)S(1)} all-to-all(bf16[2,16,2048]{2,1,0:T(8,128)(2,1)S(1)} %broadcast_in_dim.8), channel_id=1, replica_groups=mesh['grp'=2,'ep_0'=16,'ep_1'=4,'tp'=2] {'tp'}, dimensions={0} | all-to-all | bytes 262144 | tf_op jit(solution)/shard_map/all_to_all | solution.py:34
  274.8 129.9 %all-gather.11.cloned.1.call-done = bf16[1024,2050]{1,0:T(8,128)(2,1)} async-done(((bf16[16,2050]{1,0:T(8,128)(2,1)}), bf16[1024,2050]{1,0:T(8,128)(2,1)}) %all-gather.11.cloned.1.call-update) | async-done | bytes 4198416 | tf_op jit(solution)/shard_map/all_gather | solution.py:54
  404.7 3.7 fusion.31
  408.5 1.3 fusion.46
  410.5 3.7 fusion.35
  414.3 1.4 fusion.40
  419.0 13.5 %all-to-all-start.2 = ((bf16[224,2,1024]{2,0,1:T(8,128)(2,1)}), bf16[224,2,1024]{2,0,1:T(8,128)(2,1)S(1)}, u32[]{:S(2)}, u32[]{:S(2)}) async-start(bf16[224,2,1024]{2,0,1:T(8,128)(2,1)} %bitcast.75), calls=%async_computation.2 | async-start | bytes 1835008 | tf_op jit(solution)/shard_map/all_to_all | solution.py:240
  432.5 61.6 %all-gather.1 = s32[64,16,2]{1,2,0:T(2,128)S(1)} all-gather(s32[1,16,2]{1,2,0:T(2,128)S(1)} %bitcast.90), channel_id=1, replica_groups=mesh['grp'=2,'ep_0'=16,'ep_1'=4,'tp'=2] {'ep_0','ep_1'}, dimensions={0}, use_global_device_ids=true | all-gather | bytes 8320 | tf_op jit(solution)/shard_map/all_gather | solution.py:224
  495.4 3.4 fusion.27
  498.8 1.5 reshape.134
  501.2 1.4 reshape.129
  503.9 1.5 reshape.130
  505.7 22.6 %all-to-all-start.3 = ((bf16[44,2,1024]{2,0,1:T(8,128)(2,1)}), bf16[44,2,1024]{2,0,1:T(8,128)(2,1)S(1)}, u32[]{:S(2)}, u32[]{:S(2)}) async-start(bf16[44,2,1024]{2,0,1:T(8,128)(2,1)} %copy.77), calls=%async_computation.3 | async-start | bytes 393216 | tf_op jit(solution)/shard_map/all_to_all | solution.py:241
  528.2 4.4 fusion.58
  532.7 4.4 fusion.8
  537.0 9.9 %all-to-all-start.4 = ((bf16[64,16,1024]{2,1,0:T(8,128)(2,1)}), bf16[64,16,1024]{2,1,0:T(8,128)(2,1)S(1)}, u32[]{:S(2)}, u32[]{:S(2)}) async-start(bf16[64,16,1024]{2,1,0:T(8,128)(2,1)} %bitcast.20), calls=%async_computation.4 | async-start | bytes 4194304 | tf_op jit(solution)/shard_map/all_to_all | solution.py:81
  546.9 95.3 %all-to-all-done.4 = bf16[64,16,1024]{2,1,0:T(8,128)(2,1)S(1)} async-done(((bf16[64,16,1024]{2,1,0:T(8,128)(2,1)}), bf16[64,16,1024]{2,1,0:T(8,128)(2,1)S(1)}, u32[]{:S(2)}, u32[]{:S(2)}) %all-to-all-start.4) | async-done | bytes 2097184 | tf_op jit(solution)/shard_map/all_to_all | solution.py:81
  642.6 7.9 %all_to_all.68 = f32[2,8,1024]{2,1,0:T(8,128)S(1)} all-to-all(f32[2,8,1024]{2,1,0:T(8,128)S(1)} %bitcast.84), channel_id=1, replica_groups=mesh['grp'=2,'ep_0'=16,'ep_1'=4,'tp'=2] {'tp'}, dimensions={0} | all-to-all | bytes 131072 | tf_op jit(solution)/shard_map/all_to_all | solution.py:250
  (98 shorter events, 15.4 us)
Async XLA Ops:
  7.2 403.3 %copy-start = (bf16[2048,224]{0,1:T(8,128)(2,1)S(1)}, bf16[2048,224]{0,1:T(8,128)(2,1)}, u32[]{:S(2)}) copy-start(bf16[2048,224]{0,1:T(8,128)(2,1)} %param.43) | copy-start | bytes 2752516
  7.2 183.1 %all-gather.7.cloned.1.call-start = ((), (), s32[]{:S(2)}) async-start(), calls=%async_computation.6 | async-start | bytes 12779520 | tf_op jit(solution)/shard_map/all_gather | solution.py:22
  9.0 248.0 %all-gather.9.cloned.1.call-start = ((), (), s32[]{:S(2)}) async-start(), calls=%async_computation.7 | async-start | bytes 4456448 | tf_op jit(solution)/shard_map/all_gather | solution.py:44
  22.0 382.7 %all-gather.11.cloned.1.call-start = ((), (), s32[]{:S(2)}) async-start(), calls=%async_computation.8 | async-start | bytes 4526080 | tf_op jit(solution)/shard_map/all_gather | solution.py:54
  232.4 6.6 %copy-start.2 = (f32[16,16,64,64]{3,2,1,0:T(8,128)}, f32[16,16,64,64]{3,2,1,0:T(8,128)S(1)}, u32[]{:S(2)}) copy-start(f32[16,16,64,64]{3,2,1,0:T(8,128)S(1)} %multiply_add_fusion) | copy-start | bytes 12582916
  232.4 7.0 %copy-start.7 = (f32[16,64]{1,0:T(8,128)S(1)}, f32[16,64]{1,0:T(8,128)}, u32[]{:S(2)}) copy-start(f32[16,64]{1,0:T(8,128)} %param.42) | copy-start | bytes 12292
  239.0 34.5 %copy-start.4 = (bf16[16,2048]{1,0:T(8,128)(2,1)S(1)}, bf16[16,2048]{1,0:T(8,128)(2,1)}, u32[]{:S(2)}) copy-start(bf16[16,2048]{1,0:T(8,128)(2,1)} %param.25) | copy-start | bytes 196612
  239.0 34.7 %copy-start.8 = (f32[2048]{0:T(1024)S(1)}, f32[2048]{0:T(1024)}, u32[]{:S(2)}) copy-start(f32[2048]{0:T(1024)} %param.30) | copy-start | bytes 24580
  239.0 165.7 %copy-start.12 = (bf16[2048,44]{0,1:T(8,128)(2,1)S(1)}, bf16[2048,44]{0,1:T(8,128)(2,1)}, u32[]{:S(2)}) copy-start(bf16[2048,44]{0,1:T(8,128)(2,1)} %param.46) | copy-start | bytes 540676
  274.5 134.0 %copy-start.13 = (bf16[2048,44]{0,1:T(8,128)(2,1)S(1)}, bf16[2048,44]{0,1:T(8,128)(2,1)}, u32[]{:S(2)}) copy-start(bf16[2048,44]{0,1:T(8,128)(2,1)} %param.47) | copy-start | bytes 540676
  274.5 224.3 %all-gather.13.cloned.1.call-start = ((), (), s32[]{:S(2)}) async-start(), calls=%async_computation.9 | async-start | bytes 1646592 | tf_op jit(solution)/shard_map/all_gather | solution.py:65
  404.7 3.7 copy-start.3
  410.0 4.3 slice-start
  410.5 3.8 slice-start.1
  410.5 3.8 copy-start.11
  415.8 2.2 copy-start.5
  415.8 16.7 %copy-start.9 = (bf16[2048]{0:T(1024)(128)(2,1)S(1)}, bf16[2048]{0:T(1024)(128)(2,1)}, u32[]{:S(2)}) copy-start(bf16[2048]{0:T(1024)(128)(2,1)} %param.49) | copy-start | bytes 12292
  415.8 16.7 %copy-start.10 = (s32[16,2]{0,1:T(2,128)S(1)}, s32[16,2]{0,1:T(2,128)}, u32[]{:S(2)}) copy-start(s32[16,2]{0,1:T(2,128)} %param.27) | copy-start | bytes 388
  415.8 78.6 %copy-start.6 = (bf16[44,2048]{1,0:T(8,128)(2,1)S(1)}, bf16[44,2048]{1,0:T(8,128)(2,1)}, u32[]{:S(2)}) copy-start(bf16[44,2048]{1,0:T(8,128)(2,1)} %param.48) | copy-start | bytes 540676
  415.8 79.4 %slice-start.2 = ((bf16[1024,2050]{1,0:T(8,128)(2,1)}), bf16[1024,2]{1,0:T(8,128)(2,1)S(1)}, s32[]{:S(2)}) async-start(bf16[1024,2050]{1,0:T(8,128)(2,1)} %all-gather.11.cloned.1.call-done), calls=%async_computation.12 | async-start | bytes 524288 | tf_op jit(solution)/shard_map/split | solution.py:54
  419.0 86.7 %all-to-all-start.2 = ((bf16[224,2,1024]{2,0,1:T(8,128)(2,1)}), bf16[224,2,1024]{2,0,1:T(8,128)(2,1)S(1)}, u32[]{:S(2)}, u32[]{:S(2)}) async-start(bf16[224,2,1024]{2,0,1:T(8,128)(2,1)} %bitcast.75), calls=%async_computation.2 | async-start | bytes 1835008 | tf_op jit(solution)/shard_map/all_to_all | solution.py:240
  505.7 27.0 %all-to-all-start.3 = ((bf16[44,2,1024]{2,0,1:T(8,128)(2,1)}), bf16[44,2,1024]{2,0,1:T(8,128)(2,1)S(1)}, u32[]{:S(2)}, u32[]{:S(2)}) async-start(bf16[44,2,1024]{2,0,1:T(8,128)(2,1)} %copy.77), calls=%async_computation.3 | async-start | bytes 393216 | tf_op jit(solution)/shard_map/all_to_all | solution.py:241
  532.7 118.5 %copy-start.1 = (bf16[2048,224]{0,1:T(8,128)(2,1)S(1)}, bf16[2048,224]{0,1:T(8,128)(2,1)}, u32[]{:S(2)}) copy-start(bf16[2048,224]{0,1:T(8,128)(2,1)} %param.43) | copy-start | bytes 2752516
  537.0 105.3 %all-to-all-start.4 = ((bf16[64,16,1024]{2,1,0:T(8,128)(2,1)}), bf16[64,16,1024]{2,1,0:T(8,128)(2,1)S(1)}, u32[]{:S(2)}, u32[]{:S(2)}) async-start(bf16[64,16,1024]{2,1,0:T(8,128)(2,1)} %bitcast.20), calls=%async_computation.4 | async-start | bytes 4194304 | tf_op jit(solution)/shard_map/all_to_all | solution.py:81
Sparse Core Ops, SparseCore 0:
  11.0 179.2 all-gather.6
  192.1 64.8 all-gather.8
  274.6 130.0 all-gather.10
  418.1 23.4 all-gather.12
where the time goes:
time: 659 us; the launch traced here: 658 us
  waiting for transfers between devices  404 us (61%)
  blocking collectives  102 us (15%)
  matrix products  60.8 us (9%)
  starting transfers between devices  46.5 us (7%)
  other arithmetic  16.3 us (2%)
  between operations  14.3 us (2%)
  local copies, waits for them, and re-layouts  13.2 us (2%)
    all_gather x1, waiting for transfers between devices, turned_gather(): whole = lax.all_gather(both, axis, axis=0, tiled=True)  162 us
    all_gather x1, waiting for transfers between devices, side_by_side(): lax.all_gather(both, axis, axis=dim, tiled=True)  130 us
    all_to_all x1, waiting for transfers between devices, sent_and_summed(): lax.all_to_all(cut_along(value, dim, devices), axis, 0, 0, tiled=True)  95.3 us
    all_gather x1, blocking collectives, body(): lax.all_gather(chosen_specialist, EP, axis=0, tiled=True)  61.6 us
    all_to_all x1, starting transfers between devices, body(): lax.all_to_all(common_contract, 'tp', split_axis=1, concat_axis=0, tiled=...  22.6 us
    all_to_all x2, blocking collectives, from_everyone(): return lax.all_to_all(copies, axis, split_axis=0, concat_axis=0, tiled=True)  20 us
    all_gather x1, waiting for transfers between devices, whole_of(): nearer = lax.all_gather(value, axes[-1], axis=dim, tiled=True)  16.9 us
    dot_general x1, matrix products, evolve_memory(): jnp.einsum('bhvk,bhk->bhv', memory_arrays, unit_key, precision=HIGHEST)  15.4 us
  transfers between devices with their start and end apart: 7, of which 4 were waited for; matrix products, arithmetic and copies ran while one was open for 10% of the time, Pallas kernels for 0%

commit v1 on v0

--- a/solution.py
+++ b/solution.py
@@ -221,7 +221,9 @@
     ffn_in = rms_norm(residual, second_rescale).astype(jnp.bfloat16)
     all_in, all_weight, all_ids = (
         *side_by_side((ffn_in, chosen_coefficient), EP, 0, 1),
-        lax.all_gather(chosen_specialist, EP, axis=0, tiled=True),
+        jnp.concatenate(
+            lax.all_to_all(jnp.stack([chosen_specialist] * lax.axis_size(EP)), EP, 0, 0), axis=0
+        ),
     )
     column_count = specialist_switch.shape[1]
     flat_rank = lax.axis_index(EP) * tp_count + tp_rank

time: 659 us -> 599 us (0.909)
  blocking collectives: 102 us -> 39.7 us
  waiting for transfers between devices: 404 us -> 416 us
  starting transfers between devices: 46.5 us -> 36.3 us
    all_gather x1 -> x0, blocking collectives: 61.6 us -> none  [body(): lax.all_gather(chosen_specialist, EP, axis=0, tiled=True)]
    all_to_all x1, starting transfers between devices: 22.6 us -> 3.73 us  [body(): lax.all_to_all(common_contract, 'tp', split_axis=1, concat_axis=0, tiled=...]
    all_to_all x0 -> x1, waiting for transfers between devices: none -> 10.9 us  [body(): lax.all_to_all(jnp.stack([chosen_specialist] * lax.axis_size(EP)), EP, 0, 0)]
    all_to_all x0 -> x1, starting transfers between devices: none -> 10.4 us  [body(): lax.all_to_all(jnp.stack([chosen_specialist] * lax.axis_size(EP)), EP, 0, 0)]
  transfers between devices with their start and end apart: 7 -> 8, of which waited for: 4 -> 5; matrix products, arithmetic and copies ran while one was open for 10% -> 11% of each run, Pallas kernels for 0% -> 0%
where the time goes in v1:
time: 599 us; the launch traced here: 597 us
  waiting for transfers between devices  416 us (69%)
  matrix products  60.8 us (10%)
  blocking collectives  39.7 us (7%)
  starting transfers between devices  36.3 us (6%)
  other arithmetic  16.3 us (3%)
  between operations  14.3 us (2%)
  local copies, waits for them, and re-layouts  13.8 us (2%)
    all_gather x1, waiting for transfers between devices, turned_gather(): whole = lax.all_gather(both, axis, axis=0, tiled=True)  162 us
    all_gather x1, waiting for transfers between devices, side_by_side(): lax.all_gather(both, axis, axis=dim, tiled=True)  130 us
    all_to_all x1, waiting for transfers between devices, sent_and_summed(): lax.all_to_all(cut_along(value, dim, devices), axis, 0, 0, tiled=True)  96.3 us
    all_to_all x2, blocking collectives, from_everyone(): return lax.all_to_all(copies, axis, split_axis=0, concat_axis=0, tiled=True)  20 us
    all_gather x1, waiting for transfers between devices, whole_of(): nearer = lax.all_gather(value, axes[-1], axis=dim, tiled=True)  16.9 us
    dot_general x1, matrix products, evolve_memory(): jnp.einsum('bhvk,bhk->bhv', memory_arrays, unit_key, precision=HIGHEST)  15.4 us
    all_to_all x1, starting transfers between devices, body(): lax.all_to_all(specialist_contract, 'tp', split_axis=1, concat_axis=0, ti...  15.2 us
    all_gather x1, blocking collectives, whole_of(): nearer = lax.all_gather(value, axes[-1], axis=dim, tiled=True)  12.9 us
  transfers between devices with their start and end apart: 8, of which 5 were waited for; matrix products, arithmetic and copies ran while one was open for 11% of the time, Pallas kernels for 0%

profile of v1, /device:TPU:33, one launch (start us, length us, event | category | flops | bytes accessed | tf_op | source)
XLA Modules:
  0.0 597.4 jit_solution(15757787576377323111)
XLA Ops:
  7.3 1.7 pad_maximum_fusion.1
  9.1 12.9 %all_gather.19 = bf16[1024,128]{0,1:T(8,128)(2,1)} all-gather(bf16[1024,32]{0,1:T(8,128)(2,1)} %param.34), channel_id=1, replica_groups=mesh['grp'=2,'ep_0'=16,'ep_1'=4,'tp'=2] {'ep_1'}, dimensions={1}, use_global_device_ids=true | all-gather | bytes 327680 | tf_op jit(solution)/shard_map/all_gather | solution.py:44
  25.5 1.4 fusion.55
  27.0 1.4 fusion.71
  28.5 161.8 %all-gather.6.cloned.1.call-done = bf16[2048,3072]{1,0:T(8,128)(2,1)} async-done(((bf16[32,3072]{1,0:T(8,128)(2,1)}), bf16[2048,3072]{1,0:T(8,128)(2,1)}) %all-gather.6.cloned.1.call-update) | async-done | bytes 12582928 | tf_op jit(solution)/shard_map/all_gather | solution.py:22
  190.3 3.4 fusion.18
  193.7 3.4 fusion.21
  197.1 3.4 fusion.24
  200.5 6.9 %all_to_all.71 = bf16[2,16,3,2048]{3,1,2,0:T(8,128)(2,1)S(1)} all-to-all(bf16[2,16,3,2048]{3,1,2,0:T(8,128)(2,1)S(1)} %broadcast_in_dim.7), channel_id=1, replica_groups=mesh['grp'=2,'ep_0'=16,'ep_1'=4,'tp'=2] {'tp'}, dimensions={0} | all-to-all | bytes 786432 | tf_op jit(solution)/shard_map/all_to_all | solution.py:34
  208.2 15.4 %fusion.80 = f32[16,16,1,64]{3,2,1,0:T(1,128)S(1)} fusion(f32[16,16,64,1]{2,3,1,0:T(1,128)S(1)} %bitcast.82, f32[16,16,64,64]{3,2,1,0:T(8,128)} %param.26), kind=kOutput, calls=%fused_computation.96 | convolution fusion | flops 12582912 | bytes 4325376 | tf_op jit(solution)/shard_map/bhvk,bhk->bhv/dot_general | solution.py:108
  223.6 8.8 %multiply_add_fusion = f32[16,16,64,64]{3,2,1,0:T(8,128)S(1)} fusion(f32[16,16,64,64]{3,2,1,0:T(8,128)} %param.26, f32[16,16,64]{2,1,0:T(8,128)S(1)} %get-tuple-element.8, f32[16,16,64]{2,1,0:T(8,128)S(1)} %reshape.138, f32[16,16,64]{2,1,0:T(8,128)S(1)} %get-tuple-element.6, f32[16,16,64]{2,1,0:T(8,128)S(1)} %bitcast.81, f32[16,16,64]{2,1,0:T(8,128)S(1)} %mul.210), kind=kLoop, calls=%fused_computation.1 | loop fusion | flops 5242880 | bytes 8716288 | tf_op jit(solution)/shard_map/add | solution.py:110
  232.4 6.6 %fusion.81 = f32[16,16,1,64]{3,2,1,0:T(1,128)S(1)} fusion(f32[16,16,64,64]{3,2,1,0:T(8,128)S(1)} %multiply_add_fusion, bf16[16,16,64,1]{2,3,1,0:T(2,128)(2,1)S(1)} %reshape.149), kind=kOutput, calls=%fused_computation.97 | convolution fusion | flops 12582912 | bytes 4292608 | tf_op jit(solution)/shard_map/bhvk,bhk->bhv/dot_general | solution.py:114
  240.0 16.9 %all-gather.8.cloned.1.call-done = bf16[1024,2048]{0,1:T(8,128)(2,1)} async-done(((bf16[1024,128]{0,1:T(8,128)(2,1)}), bf16[1024,2048]{0,1:T(8,128)(2,1)}) %all-gather.8.cloned.1.call-update) | async-done | bytes 4194320 | tf_op jit(solution)/shard_map/all_gather | solution.py:44
  257.0 3.4 convolution_convert_fusion
  260.4 13.1 %all_to_all.72 = bf16[2,16,2048]{2,1,0:T(8,128)(2,1)S(1)} all-to-all(bf16[2,16,2048]{2,1,0:T(8,128)(2,1)S(1)} %broadcast_in_dim.8), channel_id=1, replica_groups=mesh['grp'=2,'ep_0'=16,'ep_1'=4,'tp'=2] {'tp'}, dimensions={0} | all-to-all | bytes 262144 | tf_op jit(solution)/shard_map/all_to_all | solution.py:34
  274.8 129.9 %all-gather.10.cloned.1.call-done = bf16[1024,2050]{1,0:T(8,128)(2,1)} async-done(((bf16[16,2050]{1,0:T(8,128)(2,1)}), bf16[1024,2050]{1,0:T(8,128)(2,1)}) %all-gather.10.cloned.1.call-update) | async-done | bytes 4198416 | tf_op jit(solution)/shard_map/all_gather | solution.py:54
  404.7 3.7 fusion.31
  410.5 3.7 fusion.35
  414.4 1.4 fusion.40
  418.6 10.4 %all-to-all-start.2 = ((s32[64,16,2]{1,2,0:T(2,128)}), s32[64,16,2]{1,2,0:T(2,128)S(1)}, u32[]{:S(2)}, u32[]{:S(2)}) async-start(s32[64,16,2]{1,2,0:T(2,128)} %stack.18), calls=%async_computation.2 | async-start | bytes 131072 | tf_op jit(solution)/shard_map/all_to_all | solution.py:225
  430.8 10.9 %all-to-all-done.2 = s32[64,16,2]{1,2,0:T(2,128)S(1)} async-done(((s32[64,16,2]{1,2,0:T(2,128)}), s32[64,16,2]{1,2,0:T(2,128)S(1)}, u32[]{:S(2)}, u32[]{:S(2)}) %all-to-all-start.2) | async-done | bytes 8224 | tf_op jit(solution)/shard_map/all_to_all | solution.py:225
  441.7 15.2 %all-to-all-start.3 = ((bf16[224,2,1024]{2,0,1:T(8,128)(2,1)}), bf16[224,2,1024]{2,0,1:T(8,128)(2,1)S(1)}, u32[]{:S(2)}, u32[]{:S(2)}) async-start(bf16[224,2,1024]{2,0,1:T(8,128)(2,1)} %bitcast.74), calls=%async_computation.3 | async-start | bytes 1835008 | tf_op jit(solution)/shard_map/all_to_all | solution.py:242
  457.4 3.4 fusion.27
  460.8 1.5 reshape.139
  463.1 1.4 reshape.134
  465.8 1.5 reshape.135
  467.6 3.7 all-to-all-start.4
  471.3 4.4 fusion.58
  475.7 4.4 fusion.8
  480.1 6.6 %all-to-all-start.5 = ((bf16[64,16,1024]{2,1,0:T(8,128)(2,1)}), bf16[64,16,1024]{2,1,0:T(8,128)(2,1)S(1)}, u32[]{:S(2)}, u32[]{:S(2)}) async-start(bf16[64,16,1024]{2,1,0:T(8,128)(2,1)} %bitcast.19), calls=%async_computation.5 | async-start | bytes 4194304 | tf_op jit(solution)/shard_map/all_to_all | solution.py:81
  486.7 96.3 %all-to-all-done.5 = bf16[64,16,1024]{2,1,0:T(8,128)(2,1)S(1)} async-done(((bf16[64,16,1024]{2,1,0:T(8,128)(2,1)}), bf16[64,16,1024]{2,1,0:T(8,128)(2,1)S(1)}, u32[]{:S(2)}, u32[]{:S(2)}) %all-to-all-start.5) | async-done | bytes 2097184 | tf_op jit(solution)/shard_map/all_to_all | solution.py:81
  583.3 6.9 %all_to_all.73 = f32[2,8,1024]{2,1,0:T(8,128)S(1)} all-to-all(f32[2,8,1024]{2,1,0:T(8,128)S(1)} %bitcast.83), channel_id=1, replica_groups=mesh['grp'=2,'ep_0'=16,'ep_1'=4,'tp'=2] {'tp'}, dimensions={0} | all-to-all | bytes 131072 | tf_op jit(solution)/shard_map/all_to_all | solution.py:252
  (100 shorter events, 17.3 us)
Async XLA Ops:
  7.2 403.3 %copy-start = (bf16[2048,224]{0,1:T(8,128)(2,1)S(1)}, bf16[2048,224]{0,1:T(8,128)(2,1)}, u32[]{:S(2)}) copy-start(bf16[2048,224]{0,1:T(8,128)(2,1)} %param.43) | copy-start | bytes 2752516
  7.2 183.1 %all-gather.6.cloned.1.call-start = ((), (), s32[]{:S(2)}) async-start(), calls=%async_computation.7 | async-start | bytes 12779520 | tf_op jit(solution)/shard_map/all_gather | solution.py:22
  9.0 248.0 %all-gather.8.cloned.1.call-start = ((), (), s32[]{:S(2)}) async-start(), calls=%async_computation.8 | async-start | bytes 4456448 | tf_op jit(solution)/shard_map/all_gather | solution.py:44
  22.0 382.7 %all-gather.10.cloned.1.call-start = ((), (), s32[]{:S(2)}) async-start(), calls=%async_computation.9 | async-start | bytes 4526080 | tf_op jit(solution)/shard_map/all_gather | solution.py:54
  232.4 6.6 %copy-start.2 = (f32[16,16,64,64]{3,2,1,0:T(8,128)}, f32[16,16,64,64]{3,2,1,0:T(8,128)S(1)}, u32[]{:S(2)}) copy-start(f32[16,16,64,64]{3,2,1,0:T(8,128)S(1)} %multiply_add_fusion) | copy-start | bytes 12582916
  232.4 7.0 %copy-start.7 = (f32[16,64]{1,0:T(8,128)S(1)}, f32[16,64]{1,0:T(8,128)}, u32[]{:S(2)}) copy-start(f32[16,64]{1,0:T(8,128)} %param.42) | copy-start | bytes 12292
  239.0 34.5 %copy-start.4 = (bf16[16,2048]{1,0:T(8,128)(2,1)S(1)}, bf16[16,2048]{1,0:T(8,128)(2,1)}, u32[]{:S(2)}) copy-start(bf16[16,2048]{1,0:T(8,128)(2,1)} %param.25) | copy-start | bytes 196612
  239.0 34.7 %copy-start.8 = (f32[2048]{0:T(1024)S(1)}, f32[2048]{0:T(1024)}, u32[]{:S(2)}) copy-start(f32[2048]{0:T(1024)} %param.30) | copy-start | bytes 24580
  239.0 165.7 %copy-start.12 = (bf16[2048,44]{0,1:T(8,128)(2,1)S(1)}, bf16[2048,44]{0,1:T(8,128)(2,1)}, u32[]{:S(2)}) copy-start(bf16[2048,44]{0,1:T(8,128)(2,1)} %param.46) | copy-start | bytes 540676
  274.5 134.0 %copy-start.13 = (bf16[2048,44]{0,1:T(8,128)(2,1)S(1)}, bf16[2048,44]{0,1:T(8,128)(2,1)}, u32[]{:S(2)}) copy-start(bf16[2048,44]{0,1:T(8,128)(2,1)} %param.47) | copy-start | bytes 540676
  274.5 186.3 %all-gather.12.cloned.1.call-start = ((), (), s32[]{:S(2)}) async-start(), calls=%async_computation.10 | async-start | bytes 1646592 | tf_op jit(solution)/shard_map/all_gather | solution.py:65
  404.7 3.7 copy-start.3
  410.0 4.3 slice-start
  410.5 3.8 slice-start.1
  410.5 3.8 copy-start.11
  414.3 3.6 copy-start.10
  414.3 14.7 %copy-start.9 = (bf16[2048]{0:T(1024)(128)(2,1)S(1)}, bf16[2048]{0:T(1024)(128)(2,1)}, u32[]{:S(2)}) copy-start(bf16[2048]{0:T(1024)(128)(2,1)} %param.49) | copy-start | bytes 12292
  414.3 14.7 %copy-start.6 = (bf16[44,2048]{1,0:T(8,128)(2,1)S(1)}, bf16[44,2048]{1,0:T(8,128)(2,1)}, u32[]{:S(2)}) copy-start(bf16[44,2048]{1,0:T(8,128)(2,1)} %param.48) | copy-start | bytes 540676
  415.8 14.0 %copy-start.5 = (bf16[224,2048]{1,0:T(8,128)(2,1)S(1)}, bf16[224,2048]{1,0:T(8,128)(2,1)}, u32[]{:S(2)}) copy-start(bf16[224,2048]{1,0:T(8,128)(2,1)} %param.45) | copy-start | bytes 2752516
  416.0 41.2 %slice-start.2 = ((bf16[1024,2050]{1,0:T(8,128)(2,1)}), bf16[1024,2]{1,0:T(8,128)(2,1)S(1)}, s32[]{:S(2)}) async-start(bf16[1024,2050]{1,0:T(8,128)(2,1)} %all-gather.10.cloned.1.call-done), calls=%async_computation.13 | async-start | bytes 524288 | tf_op jit(solution)/shard_map/split | solution.py:54
  418.6 23.1 %all-to-all-start.2 = ((s32[64,16,2]{1,2,0:T(2,128)}), s32[64,16,2]{1,2,0:T(2,128)S(1)}, u32[]{:S(2)}, u32[]{:S(2)}) async-start(s32[64,16,2]{1,2,0:T(2,128)} %stack.18), calls=%async_computation.2 | async-start | bytes 131072 | tf_op jit(solution)/shard_map/all_to_all | solution.py:225
  441.7 25.9 %all-to-all-start.3 = ((bf16[224,2,1024]{2,0,1:T(8,128)(2,1)}), bf16[224,2,1024]{2,0,1:T(8,128)(2,1)S(1)}, u32[]{:S(2)}, u32[]{:S(2)}) async-start(bf16[224,2,1024]{2,0,1:T(8,128)(2,1)} %bitcast.74), calls=%async_computation.3 | async-start | bytes 1835008 | tf_op jit(solution)/shard_map/all_to_all | solution.py:242
  467.6 8.2 %all-to-all-start.4 = ((bf16[44,2,1024]{2,0,1:T(8,128)(2,1)}), bf16[44,2,1024]{2,0,1:T(8,128)(2,1)S(1)}, u32[]{:S(2)}, u32[]{:S(2)}) async-start(bf16[44,2,1024]{2,0,1:T(8,128)(2,1)} %copy.92), calls=%async_computation.4 | async-start | bytes 393216 | tf_op jit(solution)/shard_map/all_to_all | solution.py:243
  475.7 115.1 %copy-start.1 = (bf16[2048,224]{0,1:T(8,128)(2,1)S(1)}, bf16[2048,224]{0,1:T(8,128)(2,1)}, u32[]{:S(2)}) copy-start(bf16[2048,224]{0,1:T(8,128)(2,1)} %param.43) | copy-start | bytes 2752516
  480.1 102.9 %all-to-all-start.5 = ((bf16[64,16,1024]{2,1,0:T(8,128)(2,1)}), bf16[64,16,1024]{2,1,0:T(8,128)(2,1)S(1)}, u32[]{:S(2)}, u32[]{:S(2)}) async-start(bf16[64,16,1024]{2,1,0:T(8,128)(2,1)} %bitcast.19), calls=%async_computation.5 | async-start | bytes 4194304 | tf_op jit(solution)/shard_map/all_to_all | solution.py:81
Sparse Core Ops, SparseCore 0:
  11.0 179.2 all-gather.5
  192.1 64.8 all-gather.7
  274.6 130.0 all-gather.9
  418.0 23.4 all-gather.11
